TPU v7x, 256 devices: a whole 4x4x8 slice. The times are simulated.
256 devices in a mesh: sp: 32 (over z, x), tp: 8 (over y, core).
Axes of the slice: x: 4, y: 4, z: 8, core: 2. Of those that a mesh axis runs over, the one named last changes fastest.
Arguments:
- tokens_in: bfloat16 [8192, 2048], P(('sp', 'tp')), may hold values from -128 to 128
- norm_gain: float32 [2048], replicated, may hold values from 0.1 to 1.9
- w_recept: bfloat16 [2048, 1024], P(None, 'tp'), may hold values from -0.125 to 0.125
- w_key_lin: bfloat16 [2048, 1024], P(None, 'tp'), may hold values from -0.125 to 0.125
- w_value_lin: bfloat16 [2048, 1024], P(None, 'tp'), may hold values from -0.125 to 0.125
- w_decay: bfloat16 [2048, 1024], P(None, 'tp'), may hold values from -0.125 to 0.125
- w_removal: bfloat16 [2048, 1024], P(None, 'tp'), may hold values from -0.125 to 0.125
- decay_base: float32 [1024], P('tp'), may hold values from -16 to -2.5
- removal_base: float32 [1024], P('tp'), may hold values from -8 to 1.5
- decay_extra: float32 [8192, 1024], P('sp', 'tp'), may hold values from -3 to 0
- initial_state: float32 [16, 64, 64], P('tp'), may hold values from -3072 to 3072
- group_gain: float32 [1024], P('tp'), may hold values from 0.1 to 1.9
- w_query: bfloat16 [2048, 1024], P(None, 'tp'), may hold values from -2 to 2
- w_key_win: bfloat16 [2048, 512], P(None, 'tp'), may hold values from -2 to 2
- w_value_win: bfloat16 [2048, 512], P(None, 'tp'), may hold values from -0.125 to 0.125
- sink_logit: float32 [16], P('tp'), may hold values from 3 to 7
- w_out_linear: bfloat16 [1024, 2048], P('tp'), may hold values from -0.1875 to 0.1875
- w_out_window: bfloat16 [1024, 2048], P('tp'), may hold values from -1 to 1
Outputs:
- mixed: bfloat16 [8192, 2048], P(('sp', 'tp'))
All inputs are finite; a program needn't handle non-finite values.
Results may differ from a plain program's by a relative error of at most 0.017.
Values may be sent and summed in bfloat16 or wider, within the bound.
No kernel may reach another device: no remote copies, remote signals or barrier semaphores. Data moves between devices by JAX's collectives and lax.ppermute only.
A program may use at most 64 MiB of HBM per device.

v0:
```python
import jax
import jax.numpy as jnp
from jax import lax
from jax.sharding import Mesh
from jax.sharding import PartitionSpec as P

HEAD_CHANNELS = 64
WINDOW = 128
SP = ("sp_0", "sp_1")
SP_TP = ("sp_0", "sp_1", "tp")


rms_eps = 1e-06
group_eps = 0.00064
key_eps = 1e-06
theta_base = 10000.0
highest_precision = lax.Precision.HIGHEST


def passed_along(array, axis, by):
    count = lax.axis_size(axis)
    pairs = [(i, i + by) for i in range(count) if 0 <= i + by < count]
    return lax.ppermute(array, axis, pairs)


def sent_to_all(array, axis):
    copies = jnp.broadcast_to(array, (lax.axis_size(axis), *array.shape))
    return lax.all_to_all(copies, axis, split_axis=0, concat_axis=0, tiled=True)


def laid_out(blocks, dim):
    blocks = jnp.moveaxis(blocks, 0, dim)
    shape = blocks.shape
    return blocks.reshape(*shape[:dim], shape[dim] * shape[dim + 1], *shape[dim + 2 :])


def gather_directly(array, axis, dim):
    blocks = sent_to_all(array, axis)
    return laid_out(blocks, dim)


def neutral_like(array, identity):
    return jax.tree.map(
        lambda part, zero: jnp.zeros_like(part) + jnp.asarray(zero, part.dtype), array, identity
    )


def collected_together(array, axis):
    leaves = jax.tree.leaves(array)
    order = sorted(range(len(leaves)), key=lambda k: -leaves[k].size)
    width = (1, *leaves[order[0]].shape)[-1]
    lines = [
        jnp.pad(leaves[k].reshape(-1), (0, -leaves[k].size % width)).reshape(-1, width)
        for k in order
    ]
    both, at, found = (lax.all_gather(jnp.concatenate(lines), axis), 0, {})
    for k, line in zip(order, lines):
        section = both[:, at : at + len(line)].reshape(len(both), -1)
        found[k] = section[:, : leaves[k].size].reshape(-1, *leaves[k].shape)
        at += len(line)
    numbers = iter(range(len(leaves)))
    return jax.tree.map(lambda _: found[next(numbers)], array)


def carried_in(array, axes, combine, identity):
    before = start = neutral_like(array, identity)
    total = array
    for axis in reversed(axes):
        count, index = (lax.axis_size(axis), lax.axis_index(axis))
        pieces = collected_together(total, axis)
        inside, total = (start, start)
        for k in range(count):
            passed = k < index
            total = combine(total, jax.tree.map(lambda part: part[k], pieces))
            inside = jax.tree.map(lambda new, old: jnp.where(passed, new, old), total, inside)
        before = combine(inside, before)
    return before


def cut_along(array, dim, count):
    before, after = (array.shape[:dim], array.shape[dim + 1 :])
    return jnp.moveaxis(array.reshape(*before, count, -1, *after), dim, 0)


def summed_on_arrival(array, axis, dim):
    blocks = cut_along(array, dim, lax.axis_size(axis))
    arrived = lax.all_to_all(blocks, axis, split_axis=0, concat_axis=0, tiled=True)
    return arrived.astype(jnp.float32).sum(axis=0)


def rotate(values, positions):
    half = HEAD_CHANNELS // 2
    inverse = theta_base ** (-jnp.arange(0, HEAD_CHANNELS, 2, dtype=jnp.float32) / HEAD_CHANNELS)
    angle = positions[:, None, None] * inverse
    cosine = jnp.cos(angle)
    sine = jnp.sin(angle)
    first = values[..., :half]
    second = values[..., half:]
    return jnp.concatenate(
        [first * cosine - second * sine, second * cosine + first * sine], axis=-1
    )


def compose(earlier, later):
    joined_map = jnp.einsum("...kj,...jl->...kl", earlier[0], later[0], precision=highest_precision)
    joined_add = (
        jnp.einsum("...vj,...jl->...vl", earlier[1], later[0], precision=highest_precision)
        + later[1]
    )
    return (joined_map, joined_add)


def window_attention(query_rows, key_rows, value_rows, sink_logit, offset):
    tok_count = query_rows.shape[0]
    kv_cols = key_rows.shape[1]
    query_heads = query_rows.shape[1] // HEAD_CHANNELS
    kv_heads = kv_cols // HEAD_CHANNELS
    group_size = query_heads // kv_heads
    positions = (offset + jnp.arange(tok_count)).astype(jnp.float32)
    query_rot = (
        rotate(
            query_rows.astype(jnp.float32).reshape(tok_count, query_heads, HEAD_CHANNELS), positions
        )
        * HEAD_CHANNELS ** (-0.5)
    ).astype(jnp.bfloat16)
    key_rot = rotate(
        key_rows.astype(jnp.float32).reshape(tok_count, kv_heads, HEAD_CHANNELS), positions
    ).astype(jnp.bfloat16)
    kv_pair = jnp.concatenate([key_rot.reshape(tok_count, kv_cols), value_rows], axis=1)
    rim_rows = passed_along(kv_pair[tok_count - WINDOW :], SP, 1)
    extended = jnp.concatenate([rim_rows, kv_pair], axis=0)
    block_count = tok_count // WINDOW
    ext_blocks = extended.reshape(block_count + 1, WINDOW, 2 * kv_cols)
    band_rows = jnp.concatenate([ext_blocks[:-1], ext_blocks[1:]], axis=1)
    banded_key = band_rows[..., :kv_cols].reshape(block_count, 2 * WINDOW, kv_heads, HEAD_CHANNELS)
    banded_value = band_rows[..., kv_cols:].reshape(
        block_count, 2 * WINDOW, kv_heads, HEAD_CHANNELS
    )
    query_block_list = query_rot.reshape(block_count, WINDOW, kv_heads, group_size, HEAD_CHANNELS)
    attention_scores = jnp.einsum(
        "bqhgd,bkhd->bhgqk", query_block_list, banded_key, preferred_element_type=jnp.float32
    )
    q_index = jnp.arange(WINDOW)
    k_index = jnp.arange(2 * WINDOW)
    relative = WINDOW + q_index[:, None] - k_index[None, :]
    near = (relative >= 0) & (relative < WINDOW)
    key_pos = offset + (jnp.arange(block_count)[:, None] - 1) * WINDOW + k_index[None, :]
    valid_mask = near[None, :, :] & (key_pos >= 0)[:, None, :]
    attention_scores = jnp.where(valid_mask[:, None, None, :, :], attention_scores, -jnp.inf)
    sinks = sink_logit.reshape(kv_heads, group_size)[None, :, :, None, None]
    row_top = jnp.maximum(jnp.max(attention_scores, axis=-1, keepdims=True), sinks)
    raised = jnp.exp(attention_scores - row_top)
    row_total = jnp.sum(raised, axis=-1, keepdims=True) + jnp.exp(sinks - row_top)
    attention_probability = (raised / row_total).astype(jnp.bfloat16)
    weighted = jnp.einsum(
        "bhgqk,bkhd->bqhgd", attention_probability, banded_value, preferred_element_type=jnp.float32
    )
    return weighted.astype(jnp.bfloat16).reshape(tok_count, query_heads * HEAD_CHANNELS)


def linear_blocks(
    receptance, lin_key, lin_value, decay_pre, removal_pre, decay_base, removal_base, decay_extra
):
    tok_count, lin_cols = receptance.shape
    head_count = lin_cols // HEAD_CHANNELS
    span_len = 32
    block_count = tok_count // span_len

    def split_heads(values):
        return values.astype(jnp.float32).reshape(block_count, span_len, head_count, HEAD_CHANNELS)

    recept_f = split_heads(receptance)
    key_full = split_heads(lin_key)
    value_full = split_heads(lin_value)
    log_decay = split_heads(-jnp.exp(decay_base + decay_pre.astype(jnp.float32)) + decay_extra)
    removal = split_heads(jax.nn.sigmoid(removal_base + removal_pre.astype(jnp.float32)))
    unit_key = key_full * lax.rsqrt(jnp.sum(key_full * key_full, axis=-1, keepdims=True) + key_eps)
    strike = unit_key * removal
    cum_log = jnp.cumsum(log_decay, axis=1)
    before = cum_log - log_decay
    order_pos = jnp.arange(span_len)
    upto = (order_pos[:, None] >= order_pos[None, :])[None, :, :, None, None]
    strict = (order_pos[:, None] > order_pos[None, :])[None, :, :, None, None]
    decay_le = jnp.exp(jnp.where(upto, cum_log[:, :, None] - cum_log[:, None, :], -jnp.inf))
    decay_lt = jnp.exp(jnp.where(strict, before[:, :, None] - cum_log[:, None, :], -jnp.inf))
    pair_form = "bthn,bshn,btshn->bhts"
    mix_beta = jnp.einsum(pair_form, -unit_key, strike, decay_lt, precision=highest_precision)
    mix_key = jnp.einsum(pair_form, -unit_key, key_full, decay_lt, precision=highest_precision)
    out_beta = jnp.einsum(pair_form, recept_f, strike, decay_le, precision=highest_precision)
    out_key = jnp.einsum(pair_form, recept_f, key_full, decay_le, precision=highest_precision)
    start_rows = jnp.swapaxes(-unit_key * jnp.exp(before), 1, 2)
    pushed = jnp.einsum("bhts,bshn->bhtn", mix_key, value_full, precision=highest_precision)
    unit_diag = jnp.eye(span_len, dtype=jnp.float32)
    solved = jax.scipy.linalg.solve_triangular(
        unit_diag - mix_beta,
        jnp.concatenate([start_rows, pushed], axis=-1),
        lower=True,
        unit_diagonal=True,
    )
    sol_state = solved[..., :HEAD_CHANNELS]
    sol_value = solved[..., HEAD_CHANNELS:]
    read_map = jnp.swapaxes(recept_f * jnp.exp(cum_log), 1, 2) + jnp.einsum(
        "bhts,bhsn->bhtn", out_beta, sol_state, precision=highest_precision
    )
    local_out = jnp.einsum(
        "bhts,bhsn->bhtn", out_beta, sol_value, precision=highest_precision
    ) + jnp.einsum("bhts,bshn->bhtn", out_key, value_full, precision=highest_precision)
    tail_decay = jnp.exp(cum_log[:, -1:] - cum_log)
    strike_tail = strike * tail_decay
    block_trans = jnp.eye(HEAD_CHANNELS, dtype=jnp.float32) * jnp.exp(cum_log[:, -1])[:, :, None, :]
    block_trans = block_trans + jnp.einsum(
        "bhtk,bthj->bhkj", sol_state, strike_tail, precision=highest_precision
    )
    block_add = jnp.einsum("bhtv,bthj->bhvj", sol_value, strike_tail, precision=highest_precision)
    block_add = block_add + jnp.einsum(
        "bthv,bthj->bhvj", value_full, key_full * tail_decay, precision=highest_precision
    )
    inc_trans, inc_add = lax.associative_scan(compose, (block_trans, block_add), axis=0)
    ident = jnp.broadcast_to(
        jnp.eye(HEAD_CHANNELS, dtype=jnp.float32), (1, head_count, HEAD_CHANNELS, HEAD_CHANNELS)
    )
    pre_trans = jnp.concatenate([ident, inc_trans[:-1]], axis=0)
    pre_add = jnp.concatenate([jnp.zeros_like(ident), inc_add[:-1]], axis=0)
    base_out = local_out + jnp.einsum(
        "bhtk,bhvk->bhtv", read_map, pre_add, precision=highest_precision
    )
    read_dev = jnp.einsum("bhtk,bhjk->bhtj", read_map, pre_trans, precision=highest_precision)
    return (base_out, read_dev, inc_trans[-1], inc_add[-1])


def per_device(
    tokens_in,
    norm_gain,
    w_recept,
    w_key_lin,
    w_value_lin,
    w_decay,
    w_removal,
    decay_base,
    removal_base,
    decay_extra,
    initial_state,
    group_gain,
    w_query,
    w_key_win,
    w_value_win,
    sink_logit,
    w_out_linear,
    w_out_window,
):
    lin_cols = w_recept.shape[1]
    query_cols = w_query.shape[1]
    kv_cols = w_key_win.shape[1]
    weight_list = (
        w_recept,
        w_key_lin,
        w_value_lin,
        w_decay,
        w_removal,
        w_query,
        w_key_win,
        w_value_win,
    )
    wide = gather_directly(tokens_in, "tp", 0).astype(jnp.float32)
    normed = (
        wide * lax.rsqrt(jnp.mean(wide * wide, axis=-1, keepdims=True) + rms_eps) * norm_gain
    ).astype(jnp.bfloat16)
    projected = jnp.concatenate(
        [
            jnp.dot(normed, weight, preferred_element_type=jnp.float32).astype(jnp.bfloat16)
            for weight in weight_list
        ],
        axis=1,
    )
    widths_list = (lin_cols, lin_cols, lin_cols, lin_cols, lin_cols, query_cols, kv_cols, kv_cols)
    pieces = []
    cursor = 0
    for width_now in widths_list:
        pieces.append(projected[:, cursor : cursor + width_now])
        cursor = cursor + width_now
    receptance, lin_key, lin_value, decay_pre, removal_pre, query_rows, key_rows, value_rows = (
        pieces
    )
    tok_count = projected.shape[0]
    head_count = lin_cols // HEAD_CHANNELS
    offset = lax.axis_index(SP) * tok_count
    win_out = window_attention(query_rows, key_rows, value_rows, sink_logit, offset)
    base_out, read_dev, dev_trans, dev_add = linear_blocks(
        receptance,
        lin_key,
        lin_value,
        decay_pre,
        removal_pre,
        decay_base,
        removal_base,
        decay_extra,
    )
    ident_state = jnp.broadcast_to(jnp.eye(HEAD_CHANNELS, dtype=jnp.float32), dev_trans.shape)
    pref_trans, pref_add = carried_in(
        (dev_trans, dev_add), SP, compose, (ident_state, jnp.zeros_like(dev_add))
    )
    entry_state = (
        jnp.einsum("hvk,hkj->hvj", initial_state, pref_trans, precision=highest_precision)
        + pref_add
    )
    reading = base_out + jnp.einsum(
        "bhtj,hvj->bhtv", read_dev, entry_state, precision=highest_precision
    )
    reading = jnp.swapaxes(reading, 1, 2).reshape(tok_count, head_count, HEAD_CHANNELS)
    centered = reading - jnp.mean(reading, axis=-1, keepdims=True)
    spread = jnp.mean(centered * centered, axis=-1, keepdims=True)
    lin_out = (
        (centered * lax.rsqrt(spread + group_eps) * group_gain.reshape(head_count, HEAD_CHANNELS))
        .reshape(tok_count, lin_cols)
        .astype(jnp.bfloat16)
    )
    summed = summed_on_arrival(
        (
            jnp.dot(lin_out, w_out_linear, preferred_element_type=jnp.float32)
            + jnp.dot(win_out, w_out_window, preferred_element_type=jnp.float32)
        ).astype(jnp.bfloat16),
        "tp",
        0,
    )
    return summed.astype(jnp.bfloat16)


def solution(mesh):
    split = Mesh(mesh.devices.reshape(8, 4, mesh.shape["tp"]), ("sp_0", "sp_1", "tp"))
    return jax.shard_map(
        per_device,
        mesh=split,
        in_specs=(
            P(SP_TP, None),
            P(),
            P(None, "tp"),
            P(None, "tp"),
            P(None, "tp"),
            P(None, "tp"),
            P(None, "tp"),
            P("tp"),
            P("tp"),
            P(SP, "tp"),
            P("tp", None, None),
            P("tp"),
            P(None, "tp"),
            P(None, "tp"),
            P(None, "tp"),
            P("tp"),
            P("tp", None),
            P("tp", None),
        ),
        out_specs=P(SP_TP, None),
        check_vma=False,
    )
```

profile of v0, /device:TPU:6, one launch (start us, length us, event | category | flops | bytes accessed | tf_op | source)
XLA Modules:
  0.0 238.7 jit_solution(8224609683553775753)
XLA Ops:
  0.0 2.1 broadcast_in_dim.49
  2.1 4.5 %all-to-all-start = ((bf16[8,32,2048]{2,1,0:T(8,128)(2,1)}), bf16[8,32,2048]{2,1,0:T(8,128)(2,1)S(1)}, u32[]{:S(2)}, u32[]{:S(2)}) async-start(bf16[8,32,2048]{2,1,0:T(8,128)(2,1)} %broadcast_in_dim.49), calls=%async_computation | async-start | bytes 2097152 | tf_op jit(solution)/shard_map/all_to_all | solution.py:28
  9.0 13.5 %all-to-all-done = bf16[8,32,2048]{2,1,0:T(8,128)(2,1)S(1)} async-done(((bf16[8,32,2048]{2,1,0:T(8,128)(2,1)}), bf16[8,32,2048]{2,1,0:T(8,128)(2,1)S(1)}, u32[]{:S(2)}, u32[]{:S(2)}) %all-to-all-start) | async-done | bytes 1048608 | tf_op jit(solution)/shard_map/all_to_all | solution.py:28
  23.9 1.5 fusion.22
  28.5 1.5 fusion.10
  30.2 1.5 fusion.16
  32.6 1.5 fusion.17
  34.8 1.8 copy_multiply_fusion.1
  36.9 5.6 %exponential_bitcast_fusion.1 = (f32[8,2,32,32,64]{4,3,1,2,0:T(8,128)S(1)}, f32[8,2,32,32,64]{4,3,1,2,0:T(8,128)}) fusion(f32[8,32,2,64]{3,1,2,0:T(8,128)S(1)} %get-tuple-element.41, f32[8,32,2,64]{3,2,1,0:T(2,128)} %copy.196, pred[32,32]{1,0:T(8,128)(4,1)} %get-tuple-element.57, f32[8,32,2,64]{3,2,1,0:T(2,128)S(1)} %copy.205, ...), kind=kLoop, calls=%fused_computation.9 | loop fusion | flops 4194304 | bytes 8783872
  42.4 22.2 %fusion.2 = (f32[8,2,32,32]{2,3,1,0:T(8,128)}, f32[8,2,32,32]{2,3,1,0:T(8,128)S(1)}, f32[8,2,32,32]{2,3,1,0:T(8,128)S(1)}, f32[8,2,32,32]{2,3,1,0:T(8,128)}) fusion(f32[8,2,32,32,64]{4,3,1,2,0:T(8,128)} %get-tuple-element.43, f32[8,2,64,32]{2,3,1,0:T(8,128)S(1)} %get-tuple-element.38, f32[8,2,64,32]{2,3,1,0:T(8,128)S(1)} %bitcast.271, ...), kind=kLoop, calls=%fused_computation.5 | loop fusion | flops 12517376 | bytes 9175040
  64.7 1.8 copy.249
  66.5 1.7 add_bitcast_fusion
  68.1 40.8 %custom-call.4 = f32[8,2,1,32,32]{3,4,2,1,0:T(8,128)} custom-call(f32[8,2,1,32,32]{4,3,2,1,0:T(8,128)} %add_bitcast_fusion), custom_call_target="InvertDiagBlocksLowerTriangular" | custom-call | tf_op jit(solution)/shard_map/jit(_solve_triangular)/vmap(vmap())/triangular_solve | solution.py:194
  109.3 1.7 fusion.37
  111.6 1.4 fusion.53
  117.6 1.3 convolution_add_fusion.2
  122.0 1.6 pad.48
  125.6 1.9 pad.41
  127.5 3.4 %pad.42 = f32[4,2,64,64]{3,2,1,0:T(8,128)} pad(f32[2,2,64,64]{3,2,1,0:T(8,128)} %pad_add_fusion.1, f32[]{:T(128)} %constant.25.clone.1), padding=1_0_1x0_0_0x0_0_0x0_0_0 | pad | bytes 196612 | tf_op jit(solution)/shard_map/pad | solution.py:218
  132.0 1.9 convolution_add_fusion.7
  133.9 3.2 %pad.162 = f32[7,2,64,64]{3,2,1,0:T(8,128)} pad(f32[4,2,64,64]{3,2,1,0:T(8,128)S(1)} %add.283, f32[]{:T(128)} %constant.25.clone.1), padding=0_0_1x0_0_0x0_0_0x0_0_0 | pad | bytes 360452
  138.2 3.2 %pad.80 = f32[7,2,64,64]{3,2,1,0:T(8,128)} pad(f32[4,2,64,64]{3,2,1,0:T(8,128)S(1)} %pad_maximum_fusion.1, f32[]{:T(128)} %constant.25.clone.1), padding=0_0_1x0_0_0x0_0_0x0_0_0 | pad | bytes 360452 | tf_op jit(solution)/shard_map/slice | solution.py:222
  141.5 3.2 %pad.49 = f32[8,2,64,64]{3,2,1,0:T(8,128)} pad(f32[4,2,64,64]{3,2,1,0:T(8,128)S(1)} %pad_maximum_fusion.1, f32[]{:T(128)} %constant.25.clone.1), padding=0_1_1x0_0_0x0_0_0x0_0_0 | pad | bytes 393220 | tf_op jit(solution)/shard_map/pad | solution.py:218
  144.7 1.7 pad_maximum_fusion
  146.4 5.1 %pad.43 = f32[8,2,64,64]{3,2,1,0:T(8,128)} pad(f32[4,2,64,64]{3,2,1,0:T(8,128)} %pad_maximum_fusion, f32[]{:T(128)} %constant.25.clone.1), padding=0_1_1x0_0_0x0_0_0x0_0_0 | pad | bytes 393220 | tf_op jit(solution)/shard_map/pad | solution.py:218
  154.3 13.6 %all-gather = f32[1024,64]{1,0:T(8,128)S(1)} all-gather(f32[256,64]{1,0:T(8,128)S(1)} %pad_maximum_fusion.4), channel_id=2, replica_groups=mesh['sp_0'=8,'sp_1'=4,'tp'=8] {'sp_1'}, dimensions={0}, use_global_device_ids=true | all-gather | bytes 327680 | tf_op jit(solution)/shard_map/all_gather | solution.py:56
  169.6 30.6 %all-gather.1 = f32[2048,64]{1,0:T(8,128)S(1)} all-gather(f32[256,64]{1,0:T(8,128)S(1)} %pad_maximum_fusion.5), channel_id=3, replica_groups=mesh['sp_0'=8,'sp_1'=4,'tp'=8] {'sp_0'}, dimensions={0}, use_global_device_ids=true | all-gather | bytes 589824 | tf_op jit(solution)/shard_map/all_gather | solution.py:56
  207.7 1.4 convolution_convert_fusion.7
  209.1 1.5 convolution_convert_fusion
  210.6 1.4 fusion.30
  212.3 2.6 %collective-permute-start = (bf16[128,128]{0,1:T(8,128)(2,1)S(1)}, bf16[128,128]{0,1:T(8,128)(2,1)S(1)}, u32[]{:S(2)}, u32[]{:S(2)}) collective-permute-start(bf16[128,128]{0,1:T(8,128)(2,1)S(1)} %slice.375), channel_id=1, source_target_pairs={{0,8},{8,16},{16,24},{24,32},{32,40},{40,48},{48,56},{56,64},{64,7... | collective-permute-start | bytes 98312 | tf_op jit(solution)/shard_map/ppermute | solution.py:23
  219.5 18.4 %all_to_all.10 = bf16[8,32,2048]{2,1,0:T(8,128)(2,1)S(1)} all-to-all(bf16[8,32,2048]{2,1,0:T(8,128)(2,1)S(1)} %bitcast.272), channel_id=1, replica_groups=mesh['sp_0'=8,'sp_1'=4,'tp'=8] {'tp'}, dimensions={0} | all-to-all | bytes 2097152 | tf_op jit(solution)/shard_map/all_to_all | solution.py:87
  (179 shorter events, 38.6 us)
Async XLA Ops:
  0.0 216.7 %copy-start = (bf16[128,2048]{1,0:T(8,128)(2,1)S(1)}, bf16[128,2048]{1,0:T(8,128)(2,1)}, u32[]{:S(2)}) copy-start(bf16[128,2048]{1,0:T(8,128)(2,1)} %param.34) | copy-start | bytes 1572868
  0.0 28.0 %copy-start.7 = (bf16[2048,128]{1,0:T(8,128)(2,1)S(1)}, bf16[2048,128]{1,0:T(8,128)(2,1)}, u32[]{:S(2)}) copy-start(bf16[2048,128]{1,0:T(8,128)(2,1)} %param.22) | copy-start | bytes 1572868
  2.1 20.4 %all-to-all-start = ((bf16[8,32,2048]{2,1,0:T(8,128)(2,1)}), bf16[8,32,2048]{2,1,0:T(8,128)(2,1)S(1)}, u32[]{:S(2)}, u32[]{:S(2)}) async-start(bf16[8,32,2048]{2,1,0:T(8,128)(2,1)} %broadcast_in_dim.49), calls=%async_computation | async-start | bytes 2097152 | tf_op jit(solution)/shard_map/all_to_all | solution.py:28
  6.6 21.4 %copy-start.16 = (f32[32]{0:T(128)}, f32[32]{0:T(128)S(1)}, u32[]{:S(2)}) copy-start(f32[32]{0:T(128)S(1)} %multiply_power_fusion) | copy-start | bytes 388
  6.6 21.4 %copy-start.14 = (f32[256]{0:T(256)}, f32[256]{0:T(256)S(1)}, u32[]{:S(2)}) copy-start(f32[256]{0:T(256)S(1)} %add_convert_fusion) | copy-start | bytes 3076
  28.5 80.4 %copy-start.2 = (bf16[8,32,2,64]{3,2,1,0:T(2,128)(2,1)}, bf16[8,32,2,64]{3,2,1,0:T(2,128)(2,1)S(1)}, u32[]{:S(2)}) copy-start(bf16[8,32,2,64]{3,2,1,0:T(2,128)(2,1)S(1)} %reshape.506) | copy-start | bytes 196612
  42.4 24.0 %copy-start.10 = (f32[32,32]{1,0:T(8,128)S(1)}, f32[32,32]{1,0:T(8,128)}, u32[]{:S(2)}) copy-start(f32[32,32]{1,0:T(8,128)} %get-tuple-element.59) | copy-start | bytes 12292
  42.4 24.0 %copy-start.13 = (pred[32,32]{1,0:T(8,128)(4,1)S(1)}, pred[32,32]{1,0:T(8,128)(4,1)}, u32[]{:S(2)}) copy-start(pred[32,32]{1,0:T(8,128)(4,1)} %get-tuple-element.58) | copy-start | bytes 3076
  42.4 70.6 %copy-start.12 = (f32[8,2,64]{2,0,1:T(8,128)S(1)}, f32[8,2,64]{2,0,1:T(8,128)}, u32[]{:S(2)}) copy-start(f32[8,2,64]{2,0,1:T(8,128)} %fusion.144) | copy-start | bytes 12292
  42.4 70.6 %copy-start.11 = (f32[8,2,64]{2,0,1:T(8,128)S(1)}, f32[8,2,64]{2,0,1:T(8,128)}, u32[]{:S(2)}) copy-start(f32[8,2,64]{2,0,1:T(8,128)} %slice_bitcast_fusion.10) | copy-start | bytes 12292
  118.9 2.3 copy-start.1
  121.9 22.8 %slice-start = ((f32[8,2,64,64]{3,2,1,0:T(8,128)}), f32[1,2,64,64]{3,2,1,0:T(8,128)S(1)}, s32[]{:S(2)}) async-start(f32[8,2,64,64]{3,2,1,0:T(8,128)} %copy-done.1), calls=%async_computation.2 | async-start | bytes 131072 | tf_op jit(solution)/shard_map/slice | solution.py:218
  138.2 66.0 %copy-start.3 = (bf16[8,32,2,64]{3,2,1,0:T(2,128)(2,1)S(1)}, bf16[8,32,2,64]{3,2,1,0:T(2,128)(2,1)}, u32[]{:S(2)}) copy-start(bf16[8,32,2,64]{3,2,1,0:T(2,128)(2,1)} %copy-done.2) | copy-start | bytes 196612
  144.7 59.6 %copy-start.5 = (f32[8,2,32,32]{2,3,1,0:T(8,128)S(1)}, f32[8,2,32,32]{2,3,1,0:T(8,128)}, u32[]{:S(2)}) copy-start(f32[8,2,32,32]{2,3,1,0:T(8,128)} %get-tuple-element.10) | copy-start | bytes 196612
  151.5 52.8 %copy-start.6 = (f32[8,2,32,64]{3,2,1,0:T(8,128)S(1)}, f32[8,2,32,64]{3,2,1,0:T(8,128)}, u32[]{:S(2)}) copy-start(f32[8,2,32,64]{3,2,1,0:T(8,128)} %fusion.53) | copy-start | bytes 393220
  151.5 53.2 %copy-start.4 = (f32[8,2,64,64]{3,2,1,0:T(8,128)S(1)}, f32[8,2,64,64]{3,2,1,0:T(8,128)}, u32[]{:S(2)}) copy-start(f32[8,2,64,64]{3,2,1,0:T(8,128)} %pad.43) | copy-start | bytes 786436
  154.3 52.2 %copy-start.9 = (f32[2,64,64]{2,1,0:T(8,128)S(1)}, f32[2,64,64]{2,1,0:T(8,128)}, u32[]{:S(2)}) copy-start(f32[2,64,64]{2,1,0:T(8,128)} %param.28) | copy-start | bytes 98308
  200.2 11.8 %copy-start.15 = (f32[256]{0:T(256)S(1)}, f32[256]{0:T(256)}, u32[]{:S(2)}) copy-start(f32[256]{0:T(256)} %copy-done.14) | copy-start | bytes 3076
  200.3 11.8 %copy-start.17 = (f32[32]{0:T(128)S(1)}, f32[32]{0:T(128)}, u32[]{:S(2)}) copy-start(f32[32]{0:T(128)} %copy-done.16) | copy-start | bytes 388
  202.1 14.6 %copy-start.19 = (f32[128]{0:T(128)S(1)}, f32[128]{0:T(128)}, u32[]{:S(2)}) copy-start(f32[128]{0:T(128)} %param.29) | copy-start | bytes 1540
  204.7 13.8 %copy-start.18 = (f32[2]{0:T(128)S(1)}, f32[2]{0:T(128)}, u32[]{:S(2)}) copy-start(f32[2]{0:T(128)} %param.33) | copy-start | bytes 28
  205.6 13.4 %copy-start.8 = (bf16[128,2048]{1,0:T(8,128)(2,1)S(1)}, bf16[128,2048]{1,0:T(8,128)(2,1)}, u32[]{:S(2)}) copy-start(bf16[128,2048]{1,0:T(8,128)(2,1)} %param.35) | copy-start | bytes 1572868
  212.3 5.8 %collective-permute-start = (bf16[128,128]{0,1:T(8,128)(2,1)S(1)}, bf16[128,128]{0,1:T(8,128)(2,1)S(1)}, u32[]{:S(2)}, u32[]{:S(2)}) collective-permute-start(bf16[128,128]{0,1:T(8,128)(2,1)S(1)} %slice.375), channel_id=1, source_target_pairs={{0,8},{8,16},{16,24},{24,32},{32,40},{40,48},{48,56},{56,64},{64,7... | collective-permute-start | bytes 98312 | tf_op jit(solution)/shard_map/ppermute | solution.py:23
where the time goes:
time: 241 us; the launch traced here: 239 us
  other arithmetic  86.6 us (36%)
  blocking collectives  62.6 us (26%)
  matrix products  33.8 us (14%)
  local copies, waits for them, and re-layouts  33.2 us (14%)
  waiting for transfers between devices  14.5 us (6%)
  starting transfers between devices  7.05 us (3%)
    all_gather x2, blocking collectives, collected_together(): both, at, found = (lax.all_gather(jnp.concatenate(lines), axis), 0, {})  44.2 us
    another operation x5, other arithmetic, linear_blocks(): jax.scipy.linalg.solve_triangular(unit_diag - mix_beta, jnp.concatenate([...  43.1 us
    unnamed x4, other arithmetic  28.6 us
    all_to_all x1, blocking collectives, summed_on_arrival(): lax.all_to_all(blocks, axis, split_axis=0, concat_axis=0, tiled=True)  18.4 us
    pad x8, local copies, waits for them, and re-layouts, linear_blocks(): lax.associative_scan(compose, (block_trans, block_add), axis=0)  15.5 us
    all_to_all x1, waiting for transfers between devices, sent_to_all(): return lax.all_to_all(copies, axis, split_axis=0, concat_axis=0, tiled=True)  13.5 us
    dot_general x8, matrix products, per_device(): jnp.dot(normed, weight, preferred_element_type=jnp.float32)  10.7 us
    dot_general x19, matrix products, compose(): jnp.einsum('...vj,...jl->...vl', earlier[1], later[0], precision=highest_...  6.45 us
  transfers between devices with their start and end apart: 2, of which 2 were waited for; matrix products, arithmetic and copies ran while one was open for 2% of the time, Pallas kernels for 0%

commit v1 on v0

v1 whole, which is shorter than its diff:
```python
import jax
import jax.numpy as jnp
from jax import lax
from jax.experimental import pallas as pl
from jax.experimental.pallas import tpu as pltpu
from jax.sharding import Mesh
from jax.sharding import PartitionSpec as P

HC = 64
WINDOW = 128
CH = 64
LANES = 128
SP = ("z", "x")
TP = ("y", "c")

rms_eps = 1e-06
group_eps = 0.00064
key_eps = 1e-06
theta_base = 10000.0
F32 = jnp.float32
BF16 = jnp.bfloat16

NN = (((1,), (0,)), ((), ()))
NT = (((1,), (1,)), ((), ()))
TN = (((0,), (0,)), ((), ()))


def dot1(a, b, dims=NN):
    return lax.dot_general(a.astype(BF16), b.astype(BF16), dims, preferred_element_type=F32)


def split(a):
    high = a.astype(BF16)
    return high, (a - high.astype(F32)).astype(BF16)


def dot3(a, b, dims=NN):
    ah, al = split(a)
    bh, bl = split(b)
    d = lambda p, q: lax.dot_general(p, q, dims, preferred_element_type=F32)
    return d(ah, bh) + (d(ah, bl) + d(al, bh))


dot_pair = dot3
dot_inv = dot3
dot_map = dot3


def head_masks(rows):
    lane = lax.broadcasted_iota(jnp.int32, (rows, LANES), 1)
    first = lane < HC
    return first


def stack2(a):
    first = head_masks(a.shape[0])
    zero = jnp.zeros_like(a)
    return jnp.concatenate([jnp.where(first, a, zero), jnp.where(first, zero, a)], axis=0)


def fold2(a):
    half = a.shape[0] // 2
    return a[:half] + a[half:]


def head_sum(a):
    first = head_masks(a.shape[0])
    low = jnp.sum(jnp.where(first, a, 0.0), axis=-1, keepdims=True)
    high = jnp.sum(jnp.where(first, 0.0, a), axis=-1, keepdims=True)
    return jnp.where(first, low, high)


def eye(count):
    row = lax.broadcasted_iota(jnp.int32, (count, count), 0)
    col = lax.broadcasted_iota(jnp.int32, (count, count), 1)
    return row == col


def level_mask(half):
    row = lax.broadcasted_iota(jnp.int32, (LANES, LANES), 0)
    col = lax.broadcasted_iota(jnp.int32, (LANES, LANES), 1)
    step = 2 * half
    same = (row // step) == (col // step)
    return same & ((row % step) >= half) & ((col % step) < half)


class Decays:
    def __init__(self, decay):
        rows = decay.shape[0]
        self.row = lax.broadcasted_iota(jnp.int32, decay.shape, 0)
        self.rows = rows
        self.half = 1
        self.incl = decay
        self.excl = jnp.ones_like(decay)
        self.tail = jnp.ones_like(decay)
        self.total = decay

    def widen(self):
        h = self.half
        second = (self.row % (2 * h)) >= h
        back = pltpu.roll(self.total, h, 0)
        ahead = pltpu.roll(self.total, self.rows - h, 0)
        sibling = jnp.where(second, back, ahead)
        lead = jnp.where(second, sibling, 1.0)
        self.incl = self.incl * lead
        self.excl = self.excl * lead
        self.tail = self.tail * jnp.where(second, 1.0, sibling)
        self.total = self.total * sibling
        self.half = 2 * h


def lin_map_kernel(
    same_ref, other_ref, gain_ref, wk_ref, wv_ref, wd_ref, wr_ref,
    db_ref, rb_ref, extra_ref, core_ref,
    normed_ref, key_ref, value_ref, strike_ref, decay_ref, sol_ref, pre_ref, map_ref,
):
    core = core_ref[0]
    count = same_ref.shape[0]
    rows = same_ref.shape[1]
    gain = gain_ref[...]
    for j in range(count):
        for ref, which in ((same_ref, core), (other_ref, 1 - core)):
            wide = ref[j].astype(F32)
            scale = lax.rsqrt(jnp.mean(wide * wide, axis=-1, keepdims=True) + rms_eps)
            at = pl.multiple_of((2 * j + which) * rows, rows)
            normed_ref[pl.ds(at, rows), :] = (wide * scale * gain).astype(BF16)
    normed = normed_ref[...]

    def project(ref):
        return jnp.dot(normed, ref[...], preferred_element_type=F32).astype(BF16)

    key_b = project(wk_ref)
    value_b = project(wv_ref)
    decay_pre = project(wd_ref).astype(F32)
    removal_pre = project(wr_ref).astype(F32)
    key = key_b.astype(F32)
    value = value_b.astype(F32)
    decay = jnp.exp(-jnp.exp(db_ref[...] + decay_pre) + extra_ref[...])
    removal = jax.nn.sigmoid(rb_ref[...] + removal_pre)
    unit = key * lax.rsqrt(head_sum(key * key) + key_eps)
    strike = unit * removal
    key_ref[...] = key_b
    value_ref[...] = value_b
    strike_ref[...] = strike
    decay_ref[...] = decay

    chunks = normed.shape[0] // CH
    ident = eye(LANES)
    prefix = None
    for b in range(chunks):
        part = slice(b * CH, (b + 1) * CH)
        u, s, k, v = -unit[part], strike[part], key[part], value[part]
        dec = Decays(decay[part])
        inverse = jnp.where(ident, 1.0, 0.0).astype(F32)
        mix_key = jnp.zeros((LANES, LANES), F32)
        while dec.half < CH:
            left = stack2(u * dec.excl)
            st = s * dec.tail
            kt = k * dec.tail
            pairs = dot_pair(left, jnp.concatenate([st, st, kt, kt], axis=0), NT)
            mask = level_mask(dec.half)
            lower = jnp.where(mask, pairs[:, :LANES], 0.0)
            mix_key = jnp.where(mask, pairs[:, LANES:], mix_key)
            if dec.half == 1:
                inverse = inverse + lower
            else:
                inverse = inverse + dot_inv(inverse, dot_inv(lower, inverse))
            dec.widen()
        v2 = stack2(v)
        right = jnp.concatenate([stack2(u * dec.excl), dot_map(mix_key, v2)], axis=1)
        sol = dot_map(inverse, right)
        sol_ref[b] = sol
        strike_tail = stack2(s * dec.tail)
        key_tail = stack2(k * dec.tail)
        both = dot_map(sol, strike_tail, TN)
        trans = both[:LANES] + jnp.where(ident, dec.total[0:1], 0.0)
        add = both[LANES:] + dot_map(v2, key_tail, TN)
        if b == 0:
            prefix = jnp.concatenate([trans, add], axis=0)
        else:
            pre_ref[b - 1] = prefix
            prefix = dot_map(prefix, trans) + jnp.concatenate([jnp.zeros_like(add), add], axis=0)
    map_ref[...] = jnp.concatenate([fold2(prefix[:LANES]), fold2(prefix[LANES:])], axis=0)


def rope(values, cosine, sine):
    lane = lax.broadcasted_iota(jnp.int32, values.shape, 1)
    low = (lane % HC) < HC // 2
    ahead = pltpu.roll(values, LANES - HC // 2, 1)
    back = pltpu.roll(values, HC // 2, 1)
    return values * cosine + jnp.where(low, -ahead, back) * sine


def qkv_kernel(normed_ref, wq_ref, wkv_ref, cos_ref, sin_ref, q_ref, kv_ref):
    normed = normed_ref[...]
    cosine = cos_ref[...]
    sine = sin_ref[...]
    q = jnp.dot(normed, wq_ref[...], preferred_element_type=F32).astype(BF16).astype(F32)
    q_ref[...] = (rope(q, cosine, sine) * HC ** (-0.5)).astype(BF16)
    kv_b = jnp.dot(normed, wkv_ref[...], preferred_element_type=F32).astype(BF16)
    kv = kv_b.astype(F32)
    first = head_masks(kv.shape[0])
    kv_ref[...] = jnp.where(first, rope(kv, cosine, sine), kv).astype(BF16)


def read_kernel(
    normed_ref, wrec_ref, key_ref, value_ref, strike_ref, decay_ref, sol_ref, pre_ref,
    base_ref, read_ref,
):
    normed = normed_ref[...]
    recept = jnp.dot(normed, wrec_ref[...], preferred_element_type=F32).astype(BF16).astype(F32)
    key = key_ref[...].astype(F32)
    value = value_ref[...].astype(F32)
    strike = strike_ref[...]
    decay = decay_ref[...]
    ident = eye(LANES)
    for b in range(normed.shape[0] // CH):
        part = slice(b * CH, (b + 1) * CH)
        r, s, k, v = recept[part], strike[part], key[part], value[part]
        dec = Decays(decay[part])
        pairs = dot_pair(stack2(r), jnp.concatenate([s, s, k, k], axis=0), NT)
        out_beta = jnp.where(ident, pairs[:, :LANES], 0.0)
        out_key = jnp.where(ident, pairs[:, LANES:], 0.0)
        while dec.half < CH:
            st = s * dec.tail
            kt = k * dec.tail
            pairs = dot_pair(stack2(r * dec.incl), jnp.concatenate([st, st, kt, kt], axis=0), NT)
            mask = level_mask(dec.half)
            out_beta = jnp.where(mask, pairs[:, :LANES], out_beta)
            out_key = jnp.where(mask, pairs[:, LANES:], out_key)
            dec.widen()
        both = dot_map(out_beta, sol_ref[b])
        read = stack2(r * dec.incl) + both[:, :LANES]
        local = both[:, LANES:] + dot_map(out_key, stack2(v))
        if b == 0:
            read_ref[part, :] = fold2(read)
            base_ref[part, :] = fold2(local)
        else:
            through = dot_map(read, pre_ref[b - 1], NT)
            read_ref[part, :] = fold2(through[:, :LANES])
            base_ref[part, :] = fold2(through[:, LANES:] + local)


def window_kernel(q_ref, kv_ref, rim_ref, sink_ref, start_ref, out_ref):
    q_all = q_ref[...].astype(F32)
    kv_all = kv_ref[...]
    first = head_masks(WINDOW)
    seen = start_ref[0]
    row = lax.broadcasted_iota(jnp.int32, (2 * WINDOW, 2 * WINDOW), 0) % WINDOW
    col = lax.broadcasted_iota(jnp.int32, (2 * WINDOW, 2 * WINDOW), 1)
    relative = WINDOW + row - col
    near = (relative >= 0) & (relative < WINDOW)
    head = lax.broadcasted_iota(jnp.int32, (2 * WINDOW, 1), 0) < WINDOW
    sinks = jnp.where(head, sink_ref[0], sink_ref[1])
    for b in range(q_all.shape[0] // WINDOW):
        q = q_all[b * WINDOW : (b + 1) * WINDOW]
        shifted = pltpu.roll(q, HC, 1)
        left = jnp.concatenate(
            [jnp.where(first, q, 0.0), jnp.where(first, shifted, 0.0)], axis=0
        ).astype(BF16)
        if b == 0:
            keys = jnp.concatenate([rim_ref[...], kv_all[:WINDOW]], axis=0)
            valid = near & (col >= seen)
        else:
            keys = kv_all[(b - 1) * WINDOW : (b + 1) * WINDOW]
            valid = near
        scores = lax.dot_general(left, keys, NT, preferred_element_type=F32)
        scores = jnp.where(valid, scores, -jnp.inf)
        top = jnp.maximum(jnp.max(scores, axis=-1, keepdims=True), sinks)
        raised = jnp.exp(scores - top)
        total = jnp.sum(raised, axis=-1, keepdims=True) + jnp.exp(sinks - top)
        prob = (raised / total).astype(BF16)
        weighted = jnp.dot(prob, keys, preferred_element_type=F32)
        low = pltpu.roll(weighted[:WINDOW], HC, 1)
        out_ref[b * WINDOW : (b + 1) * WINDOW, :] = jnp.where(
            first, low, weighted[WINDOW:]
        ).astype(BF16)


def join_kernel(maps_ref, at_ref, total_ref, before_ref):
    at = at_ref[0]
    count = maps_ref.shape[0]

    def expand(k):
        both = maps_ref[k]
        return jnp.concatenate([stack2(both[:HC]), stack2(both[HC:])], axis=0)

    total = expand(0)
    ident = jnp.where(eye(LANES), 1.0, 0.0).astype(F32)
    before = jnp.concatenate([ident, jnp.zeros_like(ident)], axis=0)
    for k in range(1, count):
        before = jnp.where(at >= k, total, before)
        later = expand(k)
        total = dot_map(total, later[:LANES])
        total = total + jnp.concatenate([jnp.zeros_like(ident), later[LANES:]], axis=0)
    before_ref[...] = before
    total_ref[...] = jnp.concatenate(
        [fold2(total[:LANES]), fold2(total[LANES:])], axis=0
    ).astype(BF16)


def final_kernel(
    maps_ref, at_ref, core_ref, before_ref, state_ref, base_ref, read_ref, gain_ref, win_ref,
    wl_ref, ww_ref, same_ref, other_ref,
):
    at = at_ref[0]
    core = core_ref[0]
    state = state_ref[...]
    for k in range(maps_ref.shape[0] - 1):
        both = maps_ref[k]
        high, low = split(state)
        moved = lax.dot_general(
            jnp.concatenate([high, low], axis=0), stack2(both[:HC]), NN,
            preferred_element_type=F32,
        )
        moved = moved[:LANES] + moved[LANES:] + stack2(both[HC:].astype(F32))
        state = jnp.where(at > k, moved, state)
    state = dot_map(state, before_ref[:LANES, :]) + before_ref[LANES:, :]
    reading = base_ref[...] + dot_map(read_ref[...], state, NT)
    centered = reading - head_sum(reading) * (1.0 / HC)
    spread = head_sum(centered * centered) * (1.0 / HC)
    lin = (centered * lax.rsqrt(spread + group_eps) * gain_ref[...]).astype(BF16)
    left = jnp.concatenate([lin, win_ref[...]], axis=1)
    weights = jnp.concatenate([wl_ref[...], ww_ref[...]], axis=0)
    term = jnp.dot(left, weights, preferred_element_type=F32).astype(BF16)
    blocks = same_ref.shape[0]
    rows = same_ref.shape[1]
    for j in range(blocks):
        even = term[2 * j * rows : (2 * j + 1) * rows]
        odd = term[(2 * j + 1) * rows : (2 * j + 2) * rows]
        same_ref[j] = jnp.where(core == 0, even, odd)
        other_ref[j] = jnp.where(core == 0, odd, even)


VM = pl.BlockSpec(memory_space=pltpu.VMEM)
SM = pl.BlockSpec(memory_space=pltpu.SMEM)


def call(kernel, outs, args, smem=(), name=None, flops=1e9):
    specs = [SM if i in smem else VM for i in range(len(args))]
    return pl.pallas_call(
        kernel,
        out_shape=outs,
        in_specs=specs,
        out_specs=jax.tree.map(lambda _: VM, outs),
        name=name,
        cost_estimate=pl.CostEstimate(flops=int(flops), transcendentals=0, bytes_accessed=1000000),
    )(*args)


def shape(dims, dtype):
    return jax.ShapeDtypeStruct(dims, dtype)


def exchanged(array, axis):
    return lax.all_to_all(array, axis, split_axis=0, concat_axis=0, tiled=True)


def copies(array, axis):
    return jnp.broadcast_to(array, (lax.axis_size(axis), *array.shape))


def per_device(
    tokens_in, norm_gain, w_recept, w_key_lin, w_value_lin, w_decay, w_removal,
    decay_base, removal_base, decay_extra, initial_state, group_gain,
    w_query, w_key_win, w_value_win, sink_logit, w_out_linear, w_out_window,
):
    model = tokens_in.shape[1]
    count = decay_extra.shape[0]
    width = decay_extra.shape[1]
    chunks = count // CH
    core = lax.axis_index("c").astype(jnp.int32).reshape(1)
    at_x = lax.axis_index("x").astype(jnp.int32).reshape(1)
    at_z = lax.axis_index("z").astype(jnp.int32).reshape(1)
    sp_index = lax.axis_index(SP)
    swap = [(0, 1), (1, 0)]

    same = exchanged(copies(tokens_in, "y"), "y")
    other = lax.ppermute(same, "c", swap)

    inverse = theta_base ** (-jnp.arange(0, HC, 2, dtype=F32) / HC)
    positions = (sp_index * count + jnp.arange(count)).astype(F32)
    angle = positions[:, None] * jnp.tile(inverse, LANES // (HC // 2))[None, :]
    cosine = jnp.cos(angle)
    sine = jnp.sin(angle)
    w_kv = jnp.concatenate([w_key_win, w_value_win], axis=1)
    zeros = jnp.zeros((HC, HC), F32)
    state0 = jnp.concatenate(
        [
            jnp.concatenate([initial_state[0], zeros], axis=1),
            jnp.concatenate([zeros, initial_state[1]], axis=1),
        ],
        axis=0,
    )

    row = lambda a: a.reshape(1, -1)
    normed, key, value, strike, decay, sol, pre, own_map = call(
        lin_map_kernel,
        (
            shape((count, model), BF16),
            shape((count, width), BF16),
            shape((count, width), BF16),
            shape((count, width), F32),
            shape((count, width), F32),
            shape((chunks, LANES, 2 * LANES), F32),
            shape((chunks - 1, 2 * LANES, LANES), F32),
            shape((2 * HC, LANES), F32),
        ),
        (
            same, other, row(norm_gain), w_key_lin, w_value_lin, w_decay, w_removal,
            row(decay_base), row(removal_base), decay_extra, core,
        ),
        smem=(10,),
        name="lin_map",
    )
    maps_x = exchanged(copies(own_map, "x"), "x")

    q_rot, kv = call(
        qkv_kernel,
        (shape((count, LANES), BF16), shape((count, LANES), BF16)),
        (normed, w_query, w_kv, cosine, sine),
        name="qkv",
    )
    steps = lax.axis_size("z") * lax.axis_size("x")
    rim = lax.ppermute(kv[count - WINDOW :], SP, [(i, i + 1) for i in range(steps - 1)])

    total, before = call(
        join_kernel,
        (shape((2 * HC, LANES), BF16), shape((2 * LANES, LANES), F32)),
        (maps_x, at_x),
        smem=(1,),
        name="join",
    )
    maps_z = exchanged(copies(total, "z"), "z")

    base, read = call(
        read_kernel,
        (shape((count, LANES), F32), shape((count, LANES), F32)),
        (normed, w_recept, key, value, strike, decay, sol, pre),
        name="read",
    )
    start = jnp.where(sp_index == 0, WINDOW, 0).astype(jnp.int32).reshape(1)
    win = call(
        window_kernel,
        shape((count, LANES), BF16),
        (q_rot, kv, rim, sink_logit, start),
        smem=(3, 4),
        name="window",
    )
    blocks = same.shape[0]
    rows = same.shape[1]
    mine, theirs = call(
        final_kernel,
        (shape((blocks, rows, model), BF16), shape((blocks, rows, model), BF16)),
        (
            maps_z, at_z, core, before, state0, base, read, row(group_gain), win,
            w_out_linear, w_out_window,
        ),
        smem=(1, 2),
        name="final",
    )
    got = lax.ppermute(theirs, "c", swap)
    pair = (mine.astype(F32) + got.astype(F32)).astype(BF16)
    arrived = exchanged(pair, "y")
    return arrived.astype(F32).sum(axis=0).astype(BF16)


def solution(mesh):
    grid = Mesh(mesh.devices.reshape(8, 4, 4, 2), ("z", "x", "y", "c"))
    return jax.shard_map(
        per_device,
        mesh=grid,
        in_specs=(
            P((*SP, *TP), None),
            P(),
            P(None, TP),
            P(None, TP),
            P(None, TP),
            P(None, TP),
            P(None, TP),
            P(TP),
            P(TP),
            P(SP, TP),
            P(TP, None, None),
            P(TP),
            P(None, TP),
            P(None, TP),
            P(None, TP),
            P(TP),
            P(TP, None),
            P(TP, None),
        ),
        out_specs=P((*SP, *TP), None),
        check_vma=False,
    )
```

time: 241 us -> 98.5 us (0.41)
  other arithmetic: 86.6 us -> 4.96 us
  blocking collectives: 62.6 us -> 12.5 us
  matrix products: 33.8 us -> 0 us
  Pallas kernels: 0 us -> 31.8 us
  local copies, waits for them, and re-layouts: 33.2 us -> 9.68 us
  starting transfers between devices: 7.05 us -> 23.4 us
    all_gather x2 -> x0, blocking collectives: 44.2 us -> none  [collected_together(): both, at, found = (lax.all_gather(jnp.concatenate(lines), axis), 0, {})]
    another operation x6 -> x0, other arithmetic: 43.3 us -> none  [the longest x5 43.1 us: linear_blocks(): jax.scipy.linalg.solve_triangular(unit_diag - mix_beta, jnp.concatenate([...]
    dot_general x61 -> x0, matrix products: 32.1 us -> none  [the longest x8 10.7 us: per_device(): jnp.dot(normed, weight, preferred_element_type=jnp.float32)]
    pallas_call x0 -> x6, Pallas kernels: none -> 31.8 us  [call(): pl.pallas_call(kernel, out_shape=outs, in_specs=specs, out_specs=jax.tree...]
    unnamed x4 -> x0, other arithmetic: 28.6 us -> none
    pad x8 -> x0, local copies, waits for them, and re-layouts: 15.5 us -> none  [linear_blocks(): lax.associative_scan(compose, (block_trans, block_add), axis=0)]
    all_to_all x1 -> x3, starting transfers between devices: 4.47 us -> 17.8 us  [exchanged(): return lax.all_to_all(array, axis, split_axis=0, concat_axis=0, tiled=True)]
    all_to_all x1, blocking collectives: 18.4 us -> 12.5 us  [exchanged(): return lax.all_to_all(array, axis, split_axis=0, concat_axis=0, tiled=True)]
  transfers between devices with their start and end apart: 2 -> 6, of which waited for: 2 -> 4; matrix products, arithmetic and copies ran while one was open for 2% -> 5% of each run, Pallas kernels for 0% -> 12%
where the time goes in v1:
time: 98.5 us; the launch traced here: 97.6 us
  Pallas kernels  31.8 us (32%)
  starting transfers between devices  23.4 us (24%)
  waiting for transfers between devices  15.2 us (15%)
  blocking collectives  12.5 us (13%)
  local copies, waits for them, and re-layouts  9.68 us (10%)
  other arithmetic  4.96 us (5%)
    pallas_call x6, Pallas kernels, call(): pl.pallas_call(kernel, out_shape=outs, in_specs=specs, out_specs=jax.tree...  31.8 us
    all_to_all x3, starting transfers between devices, exchanged(): return lax.all_to_all(array, axis, split_axis=0, concat_axis=0, tiled=True)  17.8 us
    all_to_all x1, blocking collectives, exchanged(): return lax.all_to_all(array, axis, split_axis=0, concat_axis=0, tiled=True)  12.5 us
    all_to_all x3, waiting for transfers between devices, exchanged(): return lax.all_to_all(array, axis, split_axis=0, concat_axis=0, tiled=True)  12 us
    ppermute x1, starting transfers between devices, per_device(): lax.ppermute(kv[count - WINDOW:], SP, [(i, i + 1) for i in range(steps -...  5.61 us
    broadcast_in_dim x3, local copies, waits for them, and re-layouts, copies(): return jnp.broadcast_to(array, (lax.axis_size(axis), *array.shape))  4.81 us
    unnamed x18, local copies, waits for them, and re-layouts  4.01 us
    ppermute x1, waiting for transfers between devices, per_device(): got = lax.ppermute(theirs, 'c', swap)  2.12 us
  transfers between devices with their start and end apart: 6, of which 4 were waited for; matrix products, arithmetic and copies ran while one was open for 5% of the time, Pallas kernels for 12%

profile of v1, /device:TPU:6, one launch (start us, length us, event | category | flops | bytes accessed | tf_op | source)
XLA Modules:
  0.0 97.6 jit_solution(12631347619575965037)
XLA Ops:
  0.0 1.8 %broadcast_in_dim.11 = bf16[4,32,2048]{2,1,0:T(8,128)(2,1)} broadcast(bf16[32,2048]{1,0:T(8,128)(2,1)} %param.18), dimensions={1,2} | broadcast | bytes 655360 | tf_op jit(solution)/shard_map/broadcast_in_dim | solution.py:360
  1.8 4.6 %all-to-all-start = ((bf16[4,32,2048]{2,1,0:T(8,128)(2,1)}), bf16[4,32,2048]{2,1,0:T(8,128)(2,1)S(1)}, u32[]{:S(2)}, u32[]{:S(2)}) async-start(bf16[4,32,2048]{2,1,0:T(8,128)(2,1)} %broadcast_in_dim.11), calls=%async_computation | async-start | bytes 1048576 | tf_op jit(solution)/shard_map/all_to_all | solution.py:356
  6.4 0.3 copy.20
  6.6 0.7 copy-done.2
  7.3 0.3 copy.19
  7.6 8.2 %all-to-all-done.same_ref = bf16[4,32,2048]{2,1,0:T(8,128)(2,1)S(1)} async-done(((bf16[4,32,2048]{2,1,0:T(8,128)(2,1)}), bf16[4,32,2048]{2,1,0:T(8,128)(2,1)S(1)}, u32[]{:S(2)}, u32[]{:S(2)}) %all-to-all-start) | async-done | bytes 524320 | tf_op jit(solution)/shard_map/all_to_all | solution.py:356
  15.9 0.1 mul.36
  16.0 0.7 select_maximum_fusion.state_ref
  16.7 1.1 %collective-permute-done.other_ref = bf16[4,32,2048]{2,1,0:T(8,128)(2,1)S(1)} collective-permute-done((bf16[4,32,2048]{2,1,0:T(8,128)(2,1)S(1)}, bf16[4,32,2048]{2,1,0:T(8,128)(2,1)S(1)}, u32[]{:S(2)}, u32[]{:S(2)}) %collective-permute-start) | collective-permute-done | bytes 524320 | tf_op jit(solution)/shard_map/ppermute | solution.py:379
  17.8 0.8 copy-done.6
  18.5 13.8 %lin_map.1 = (bf16[256,2048]{1,0:T(8,128)(2,1)}, bf16[256,128]{1,0:T(8,128)(2,1)}, bf16[256,128]{1,0:T(8,128)(2,1)}, f32[256,128]{1,0:T(8,128)}, f32[256,128]{1,...) custom-call(bf16[4,32,2048]{2,1,0:T(8,128)(2,1)} %copy-done, ...), custom_call_target="tpu_custom_call" | custom-call | flops 1000000000 | bytes 1000000 | tf_op jit(solution)/shard_map/lin_map/pallas_call | solution.py:341
  32.4 1.6 %broadcast_in_dim.12 = f32[4,128,128]{2,1,0:T(8,128)} broadcast(f32[128,128]{1,0:T(8,128)} %get-tuple-element.21), dimensions={1,2} | broadcast | bytes 327680 | tf_op jit(solution)/shard_map/broadcast_in_dim | solution.py:360
  33.9 4.8 %all-to-all-start.1 = ((f32[4,128,128]{2,1,0:T(8,128)}), f32[4,128,128]{2,1,0:T(8,128)S(1)}, u32[]{:S(2)}, u32[]{:S(2)}) async-start(f32[4,128,128]{2,1,0:T(8,128)} %broadcast_in_dim.12), calls=%async_computation.1 | async-start | bytes 524288 | tf_op jit(solution)/shard_map/all_to_all | solution.py:356
  38.7 1.1 %pad_maximum_fusion.wkv_ref = bf16[2048,128]{1,0:T(8,128)(2,1)} fusion(bf16[2048,64]{1,0:T(8,128)(2,1)S(1)} %copy.20, bf16[2048,64]{1,0:T(8,128)(2,1)S(1)} %copy.19), kind=kLoop, calls=%fused_computation.1 | loop fusion | flops 1048576 | bytes 1048576 | tf_op jit(solution)/shard_map/concatenate | solution.py:386
  39.8 3.8 %all-to-all-done.1.maps_ref = f32[4,128,128]{2,1,0:T(8,128)S(1)} async-done(((f32[4,128,128]{2,1,0:T(8,128)}), f32[4,128,128]{2,1,0:T(8,128)S(1)}, u32[]{:S(2)}, u32[]{:S(2)}) %all-to-all-start.1) | async-done | bytes 262176 | tf_op jit(solution)/shard_map/all_to_all | solution.py:356
  43.6 0.7 copy-done.4
  44.3 2.1 %join.1 = (bf16[128,128]{1,0:T(8,128)(2,1)}, f32[256,128]{1,0:T(8,128)}) custom-call(f32[4,128,128]{2,1,0:T(8,128)} %copy-done.4, s32[1]{0:T(128)} %bitcast.4.at_ref), custom_call_target="tpu_custom_call" | custom-call | flops 1000000000 | bytes 1000000 | tf_op jit(solution)/shard_map/join/pallas_call | solution.py:341
  46.5 1.5 %broadcast_in_dim.13 = bf16[8,128,128]{2,1,0:T(8,128)(2,1)} broadcast(bf16[128,128]{1,0:T(8,128)(2,1)} %get-tuple-element.22), dimensions={1,2} | broadcast | bytes 294912 | tf_op jit(solution)/shard_map/broadcast_in_dim | solution.py:360
  47.9 8.5 %all-to-all-start.2 = ((bf16[8,128,128]{2,1,0:T(8,128)(2,1)}), bf16[8,128,128]{2,1,0:T(8,128)(2,1)S(1)}, u32[]{:S(2)}, u32[]{:S(2)}) async-start(bf16[8,128,128]{2,1,0:T(8,128)(2,1)} %broadcast_in_dim.13), calls=%async_computation.2 | async-start | bytes 524288 | tf_op jit(solution)/shard_map/all_to_all | solution.py:356
  56.4 1.2 %multiply_sine_fusion = (f32[256,128]{1,0:T(8,128)}, f32[256,128]{1,0:T(8,128)}) fusion(f32[128]{0:T(128)S(1)} %mul.36, f32[256]{0:T(256)S(1)} %add_convert_fusion.1), kind=kLoop, calls=%fused_computation.2 | loop fusion | flops 32768 | bytes 263680 | tf_op jit(solution)/shard_map/sin | solution.py:385
  57.6 3.0 %qkv.1 = (bf16[256,128]{1,0:T(8,128)(2,1)}, bf16[256,128]{1,0:T(8,128)(2,1)}) custom-call(bf16[256,2048]{1,0:T(8,128)(2,1)} %get-tuple-element.24.normed_ref, bf16[2048,128]{1,0:T(8,128)(2,1)} %wq_ref.1, bf16[2048,128]{1,0:T(8,128)(2,1)} %pad_maximum_fusion.wkv_ref, f32[256,128]{1,0:T(8,128)} %get-tuple-element.40.cos_ref, f32[256,128]{1,0:T(8,128)} %get-tuple-element.39.sin_ref), custom_call_target="tpu_custom_call" | custom-call | flops 1000000000 | bytes 1000000 | tf_op jit(solution)/shard_map/qkv/pallas_call | solution.py:341
  60.6 0.8 slice.11
  61.4 5.6 %collective-permute-start.1 = (bf16[128,128]{1,0:T(8,128)(2,1)S(1)}, bf16[128,128]{1,0:T(8,128)(2,1)S(1)}, u32[]{:S(2)}, u32[]{:S(2)}) collective-permute-start(bf16[128,128]{1,0:T(8,128)(2,1)S(1)} %slice.11), channel_id=1, source_target_pairs={{0,8},{8,16},{16,24},{24,32},{32,40},{40,48},{48,56},{56,64},{64,7... | collective-permute-start | bytes 98312 | tf_op jit(solution)/shard_map/ppermute | solution.py:425
  67.0 5.9 %read.1 = (f32[256,128]{1,0:T(8,128)}, f32[256,128]{1,0:T(8,128)}) custom-call(bf16[256,2048]{1,0:T(8,128)(2,1)} %get-tuple-element.24.normed_ref, bf16[2048,128]{1,0:T(8,128)(2,1)} %wrec_ref.1, bf16[256,128]{1,0:T(8,128)(2,1)} %get-tuple-element.25.key_ref, bf16[256,128]{1,0:T(8,128)(2,1)} %get-tuple-element.26.value_ref, ...), custom_call_target="tpu_custom_call" | custom-call | flops 1000000000 | bytes 1000000 | tf_op jit(solution)/shard_map/read/pallas_call | solution.py:341
  72.9 0.6 copy-done.7
  73.5 2.5 %window.1.win_ref = bf16[256,128]{1,0:T(8,128)(2,1)} custom-call(bf16[256,128]{1,0:T(8,128)(2,1)} %get-tuple-element.33.q_ref, bf16[256,128]{1,0:T(8,128)(2,1)} %get-tuple-element.34.kv_ref, bf16[128,128]{1,0:T(8,128)(2,1)} %copy-done.7, f32[2]{0:T(128)} %sink_ref.1, s32[1]{0:T(128)} %bitcast.9.start_ref), custom_call_target="tpu_custom_call" | custom-call | flops 1000000000 | bytes 1000000 | tf_op jit(solution)/shard_map/window/pallas_call | solution.py:341
  75.9 0.7 copy-done.3
  76.6 4.5 %final.1 = (bf16[4,32,2048]{2,1,0:T(8,128)(2,1)}, bf16[4,32,2048]{2,1,0:T(8,128)(2,1)}) custom-call(bf16[8,128,128]{2,1,0:T(8,128)(2,1)} %copy-done.3, s32[1]{0:T(128)} %bitcast.5.at_ref, s32[1]{0:T(128)} %bitcast.3.core_ref, f32[256,128]{1,0:T(8,128)} %get-tuple-element.23.before_ref, f32[128,128]{1,0:T(8,128)} %select_maximum_fusion.state_ref, ...), custom_call_target="tpu_custom_call" | custom-call | flops 1000000000 | bytes 1000000 | tf_op jit(solution)/shard_map/final/pallas_call | solution.py:341
  81.1 2.1 %collective-permute-done.2 = bf16[4,32,2048]{2,1,0:T(8,128)(2,1)S(1)} collective-permute-done((bf16[4,32,2048]{2,1,0:T(8,128)(2,1)}, bf16[4,32,2048]{2,1,0:T(8,128)(2,1)S(1)}, u32[]{:S(2)}, u32[]{:S(2)}) %collective-permute-start.2) | collective-permute-done | bytes 524320 | tf_op jit(solution)/shard_map/ppermute | solution.py:462
  83.2 1.2 %add_convert_fusion = bf16[4,32,2048]{2,1,0:T(8,128)(2,1)S(1)} fusion(bf16[4,32,2048]{2,1,0:T(8,128)(2,1)S(1)} %collective-permute-done.2, bf16[4,32,2048]{2,1,0:T(8,128)(2,1)} %get-tuple-element.35), kind=kLoop, calls=%fused_computation | loop fusion | flops 1048576 | bytes 1572864 | tf_op jit(solution)/shard_map/convert_element_type | solution.py:463
  84.4 12.5 %all_to_all.20 = bf16[4,32,2048]{2,1,0:T(8,128)(2,1)S(1)} all-to-all(bf16[4,32,2048]{2,1,0:T(8,128)(2,1)S(1)} %add_convert_fusion), channel_id=1, replica_groups=mesh['z'=8,'x'=4,'y'=4,'c'=2] {'y'}, dimensions={0} | all-to-all | bytes 1048576 | tf_op jit(solution)/shard_map/all_to_all | solution.py:356
  96.9 0.7 reduce_sum.12
  (19 shorter events, 0.1 us)
Async XLA Ops:
  1.8 4.6 %copy-start.1 = (bf16[2048,64]{0,1:T(8,128)(2,1)S(1)}, bf16[2048,64]{0,1:T(8,128)(2,1)}, u32[]{:S(2)}) copy-start(bf16[2048,64]{0,1:T(8,128)(2,1)} %param.32) | copy-start | bytes 786436
  1.8 14.1 %all-to-all-start = ((bf16[4,32,2048]{2,1,0:T(8,128)(2,1)}), bf16[4,32,2048]{2,1,0:T(8,128)(2,1)S(1)}, u32[]{:S(2)}, u32[]{:S(2)}) async-start(bf16[4,32,2048]{2,1,0:T(8,128)(2,1)} %broadcast_in_dim.11), calls=%async_computation | async-start | bytes 1048576 | tf_op jit(solution)/shard_map/all_to_all | solution.py:356
  6.4 1.0 copy-start.2
  7.3 8.6 %copy-start.5 = (f32[2,64,64]{2,1,0:T(8,128)S(1)}, f32[2,64,64]{2,1,0:T(8,128)}, u32[]{:S(2)}) copy-start(f32[2,64,64]{2,1,0:T(8,128)} %param.28) | copy-start | bytes 98308
  15.8 1.9 %copy-start = (bf16[4,32,2048]{2,1,0:T(8,128)(2,1)}, bf16[4,32,2048]{2,1,0:T(8,128)(2,1)S(1)}, u32[]{:S(2)}) copy-start(bf16[4,32,2048]{2,1,0:T(8,128)(2,1)S(1)} %all-to-all-done.same_ref) | copy-start | bytes 1572868
  15.8 1.9 %collective-permute-start = (bf16[4,32,2048]{2,1,0:T(8,128)(2,1)S(1)}, bf16[4,32,2048]{2,1,0:T(8,128)(2,1)S(1)}, u32[]{:S(2)}, u32[]{:S(2)}) collective-permute-start(bf16[4,32,2048]{2,1,0:T(8,128)(2,1)S(1)} %all-to-all-done.same_ref), channel_id=1, source_target_pairs={{0,1},{1,0},{2,3},{3,2},{4,5},{5,4},{6,7},{7,6},{8,9},{9,8},{10,11... | collective-permute-start | bytes 1572872 | tf_op jit(solution)/shard_map/ppermute | solution.py:379
  17.7 0.8 copy-start.6
  33.9 9.7 %all-to-all-start.1 = ((f32[4,128,128]{2,1,0:T(8,128)}), f32[4,128,128]{2,1,0:T(8,128)S(1)}, u32[]{:S(2)}, u32[]{:S(2)}) async-start(f32[4,128,128]{2,1,0:T(8,128)} %broadcast_in_dim.12), calls=%async_computation.1 | async-start | bytes 524288 | tf_op jit(solution)/shard_map/all_to_all | solution.py:356
  43.6 0.7 copy-start.4
  47.9 28.0 %all-to-all-start.2 = ((bf16[8,128,128]{2,1,0:T(8,128)(2,1)}), bf16[8,128,128]{2,1,0:T(8,128)(2,1)S(1)}, u32[]{:S(2)}, u32[]{:S(2)}) async-start(bf16[8,128,128]{2,1,0:T(8,128)(2,1)} %broadcast_in_dim.13), calls=%async_computation.2 | async-start | bytes 524288 | tf_op jit(solution)/shard_map/all_to_all | solution.py:356
  61.4 11.5 %collective-permute-start.1 = (bf16[128,128]{1,0:T(8,128)(2,1)S(1)}, bf16[128,128]{1,0:T(8,128)(2,1)S(1)}, u32[]{:S(2)}, u32[]{:S(2)}) collective-permute-start(bf16[128,128]{1,0:T(8,128)(2,1)S(1)} %slice.11), channel_id=1, source_target_pairs={{0,8},{8,16},{16,24},{24,32},{32,40},{40,48},{48,56},{56,64},{64,7... | collective-permute-start | bytes 98312 | tf_op jit(solution)/shard_map/ppermute | solution.py:425
  72.9 0.6 copy-start.7
  75.9 0.7 copy-start.3
  81.1 2.1 %collective-permute-start.2 = (bf16[4,32,2048]{2,1,0:T(8,128)(2,1)}, bf16[4,32,2048]{2,1,0:T(8,128)(2,1)S(1)}, u32[]{:S(2)}, u32[]{:S(2)}) collective-permute-start(bf16[4,32,2048]{2,1,0:T(8,128)(2,1)} %get-tuple-element.36), channel_id=1, source_target_pairs={{0,1},{1,0},{2,3},{3,2},{4,5},{5,4},{6,7},{7,6},{8,9},{9,8},{10,11... | collective-permute-start | bytes 1572872 | tf_op jit(solution)/shard_map/ppermute | solution.py:462
